TPU v7x, 32 devices: a whole 2x2x4 slice. The times are simulated.
32 devices in a mesh: sp: 16 (over z, y, x), tp: 2 (over core).
Axes of the slice: x: 2, y: 2, z: 4, core: 2. Of those that a mesh axis runs over, the one named last changes fastest.
Arguments:
- tokens: bfloat16 [2048, 2048], P('sp'), may hold values from -6 to 6
- input_norm_gain: float32 [2048], replicated, may hold values from 0.1 to 1.9
- delta_query_weight: bfloat16 [2048, 1024], P('sp', 'tp'), may hold values from -0.125 to 0.125
- delta_key_weight: bfloat16 [2048, 1024], P('sp', 'tp'), may hold values from -0.125 to 0.125
- delta_value_weight: bfloat16 [2048, 1024], P('sp', 'tp'), may hold values from -0.125 to 0.125
- gate_weight: bfloat16 [2048, 4, 16], replicated, may hold values from -0.125 to 0.125
- head_decay_params: float32 [2, 16], P(None, 'tp'), may hold values from -20 to 1
- log_decay_increments: float32 [16, 2048], P('tp', 'sp'), may hold values from -2 to 0
- starting_state: float32 [2, 16, 64, 64], P(None, 'tp'), may hold values from -1.5 to 1.5
- delta_norm_gain: float32 [64], replicated, may hold values from 0.1 to 1.9
- attention_query_weight: bfloat16 [2048, 1024], P('sp', 'tp'), may hold values from -1 to 1
- attention_key_weight: bfloat16 [2048, 512], P('sp', 'tp'), may hold values from -64 to 64
- attention_value_weight: bfloat16 [2048, 512], P('sp', 'tp'), may hold values from -0.125 to 0.125
- sink: float32 [16], P('tp'), may hold values from -1 to 3
- delta_output_weight: bfloat16 [1024, 2048], P('tp'), may hold values from -0.125 to 0.125
- attention_output_weight: bfloat16 [1024, 2048], P('tp'), may hold values from -0.125 to 0.125
Outputs:
- mixed: bfloat16 [2048, 2048], P(('sp', 'tp'))
All inputs are finite; a program needn't handle non-finite values.
Results may differ from a plain program's by a relative error of at most 0.018.
Values may be sent and summed in bfloat16 or wider, within the bound.
A program may use at most 128 MiB of HBM per device.

v0:
```python
import jax
import jax.numpy as jnp
from jax import lax
from jax.sharding import PartitionSpec as P

ATTN_HEADS = 16
HEAD = 64
WINDOW = 128
BLOCK = 64


EPS = 1e-06


def extended(block, sides, width):
    for axis, dim in sides:
        count = lax.axis_size(axis)
        forward = [(i, i + 1) for i in range(count - 1)]
        backward = [(target, source) for source, target in forward]
        low = lax.ppermute(
            lax.slice_in_dim(block, block.shape[dim] - width, None, axis=dim), axis, forward
        )
        high = lax.ppermute(lax.slice_in_dim(block, 0, width, axis=dim), axis, backward)
        block = jnp.concatenate([low, block, high], axis=dim)
    return block


def outer_product(spec, left, right):
    return jnp.einsum(spec, left, right, precision=lax.Precision.HIGHEST)


def unit_lower_inverse(lower):
    width = lower.shape[-1]
    inverse = jnp.eye(width, dtype=lower.dtype) - lower
    power = lower
    for turn in range(width.bit_length() - 2):
        power = outer_product("...ij,...jk->...ik", power, power)
        inverse = inverse + outer_product("...ij,...jk->...ik", inverse, power)
    return inverse


def block_terms(query_rows, keys, values, decay, strength):
    width = decay.shape[-1]
    summed_output = jnp.cumsum(decay, axis=-1)
    index = jnp.arange(width)
    inclusive = index[:, None] >= index[None, :]
    strict = index[:, None] > index[None, :]
    spread = summed_output[..., :, None] - summed_output[..., None, :]
    weights = jnp.where(inclusive, jnp.exp(jnp.where(inclusive, spread, 0.0)), 0.0)
    scaled_keys = keys * strength[..., None]
    lower = jnp.where(strict, outer_product("...ik,...jk->...ij", scaled_keys, keys) * weights, 0.0)
    inverse = unit_lower_inverse(lower)
    state_update = outer_product("...ij,...jv->...iv", inverse, values * strength[..., None])
    delta_correction = outer_product(
        "...ij,...jk->...ik", inverse, scaled_keys * jnp.exp(summed_output)[..., None]
    )
    mixing_output = outer_product("...ik,...jk->...ij", query_rows, keys) * weights
    return (summed_output, state_update, delta_correction, mixing_output)


def local_maps(query_rows, keys, values, decay, strength):
    heads, length, width = query_rows.shape
    count = length // BLOCK

    def split(array):
        return jnp.moveaxis(array.reshape((heads, count, BLOCK) + array.shape[2:]), 1, 0)

    block_queries = split(query_rows)
    block_keys = split(keys)
    summed_output, state_update, delta_correction, mixing_output = block_terms(
        block_queries, block_keys, split(values), split(decay), split(strength)
    )
    final_state = summed_output[..., -1]
    carried_state = block_keys * jnp.exp(final_state[..., None] - summed_output)[..., None]
    identity = jnp.broadcast_to(jnp.eye(width, dtype=jnp.float32), (heads, width, width))
    block_maps = jnp.exp(final_state)[..., None, None] * identity - outer_product(
        "...bk,...bj->...kj", carried_state, delta_correction
    )
    block_adds = outer_product("...bk,...bv->...kv", carried_state, state_update)

    def compose(carry, item):
        matrix, offset = carry
        block_map, block_add = item
        return (
            (
                outer_product("hij,hjk->hik", block_map, matrix),
                outer_product("hij,hjk->hik", block_map, offset) + block_add,
            ),
            None,
        )

    totals, unused = lax.scan(
        compose, (identity, jnp.zeros_like(identity)), (block_maps, block_adds)
    )
    return (
        (
            block_queries,
            summed_output,
            state_update,
            delta_correction,
            mixing_output,
            carried_state,
        ),
        totals,
    )


def emit_outputs(start, blocks):

    def advance(running_state, item):
        query_rows, summed_output, state_update, delta_correction, mixing_output, carried_state = (
            item
        )
        fresh_values = state_update - outer_product("cpj,cjl->cpl", delta_correction, running_state)
        layer_output = outer_product(
            "cpj,cjl->cpl", query_rows * jnp.exp(summed_output)[..., None], running_state
        ) + outer_product("xgb,xbq->xgq", mixing_output, fresh_values)
        final_state = summed_output[:, -1]
        running_state = running_state * jnp.exp(final_state)[:, None, None] + outer_product(
            "tmn,tml->tnl", carried_state, fresh_values
        )
        return (running_state, layer_output)

    unused, outputs = lax.scan(advance, start, blocks)
    count, heads, length, width = outputs.shape
    return jnp.moveaxis(outputs, 0, 1).reshape(heads, count * length, width)


def reverse(array):
    return jnp.flip(array, axis=1)


def heads_first(array):
    rows = array.shape[0]
    return jnp.transpose(array.astype(jnp.float32).reshape(rows, -1, HEAD), (1, 0, 2))


def unit_rows(array):
    return array * lax.rsqrt(jnp.sum(array * array, axis=-1, keepdims=True) + EPS)


def on_device(
    tokens,
    input_norm_gain,
    delta_query_weight,
    delta_key_weight,
    delta_value_weight,
    gate_weight,
    head_decay_params,
    log_decay_increments,
    starting_state,
    delta_norm_gain,
    attention_query_weight,
    attention_key_weight,
    attention_value_weight,
    sink,
    delta_output_weight,
    attention_output_weight,
):
    tok_rows = tokens.shape[0]
    wide = tokens.astype(jnp.float32)
    normed = (
        wide * lax.rsqrt(jnp.mean(wide * wide, axis=-1, keepdims=True) + EPS) * input_norm_gain
    ).astype(jnp.bfloat16)
    pieces = (
        lax.all_gather(delta_query_weight, "sp", axis=0, tiled=True),
        lax.all_gather(delta_key_weight, "sp", axis=0, tiled=True),
        lax.all_gather(delta_value_weight, "sp", axis=0, tiled=True),
        lax.all_gather(attention_query_weight, "sp", axis=0, tiled=True),
        lax.all_gather(attention_key_weight, "sp", axis=0, tiled=True),
        lax.all_gather(attention_value_weight, "sp", axis=0, tiled=True),
    )
    sums = tuple((jnp.dot(normed, piece, preferred_element_type=jnp.float32) for piece in pieces))
    delta_query, delta_key, delta_value, attn_query, attn_key, attn_value = tuple(
        (total.astype(jnp.bfloat16) for total in sums)
    )
    heads_here = delta_query_weight.shape[1] // HEAD
    first_head = lax.axis_index("tp") * heads_here
    gate_columns = lax.dynamic_slice_in_dim(gate_weight, first_head, heads_here, 2).reshape(
        gate_weight.shape[0], 4 * heads_here
    )
    gate_values = jnp.dot(normed, gate_columns, preferred_element_type=jnp.float32).reshape(
        tok_rows, 4, heads_here
    )
    query_rows = unit_rows(heads_first(delta_query)) * HEAD ** (-0.5)
    keys = unit_rows(heads_first(delta_key))
    values = heads_first(delta_value)
    decay_rates = jnp.exp(head_decay_params[0])[:, None]
    onward_decay_factor = (
        -decay_rates * jax.nn.softplus(gate_values[:, 0, :].T) + log_decay_increments
    )
    reverse_decay_factor = (
        -decay_rates * jax.nn.softplus(gate_values[:, 1, :].T) + log_decay_increments
    )
    forward_strength = jax.nn.sigmoid(gate_values[:, 2, :].T + head_decay_params[1][:, None])
    backward_strength = jax.nn.sigmoid(gate_values[:, 3, :].T + head_decay_params[1][:, None])
    forward_blocks, forward_map = local_maps(
        query_rows, keys, values, onward_decay_factor, forward_strength
    )
    backward_blocks, backward_map = local_maps(
        reverse(query_rows),
        reverse(keys),
        reverse(values),
        reverse(reverse_decay_factor),
        reverse(backward_strength),
    )
    stacked = jnp.stack([forward_map[0], forward_map[1], backward_map[0], backward_map[1]], axis=1)[
        None
    ]
    every = lax.all_gather(stacked.astype(jnp.bfloat16), "sp", axis=0, tiled=True).astype(
        stacked.dtype
    )
    here = lax.axis_index("sp")
    places = jnp.arange(every.shape[0], dtype=jnp.int32)

    def forward_apply(running_state, item):
        place, maps = item
        moved = outer_product("hij,hjk->hik", maps[:, 0], running_state) + maps[:, 1]
        return (jnp.where(place < here, moved, running_state), None)

    def backward_apply(running_state, item):
        place, maps = item
        moved = outer_product("hij,hjk->hik", maps[:, 2], running_state) + maps[:, 3]
        return (jnp.where(place > here, moved, running_state), None)

    forward_start, unused = lax.scan(forward_apply, starting_state[0], (places, every))
    backward_start, unused = lax.scan(
        backward_apply, starting_state[1], (places, every), reverse=True
    )
    forward_out = emit_outputs(forward_start, forward_blocks)
    backward_out = reverse(emit_outputs(backward_start, backward_blocks))
    both = forward_out + backward_out
    normal_out = (
        both * lax.rsqrt(jnp.mean(both * both, axis=-1, keepdims=True) + EPS) * delta_norm_gain
    )
    delta_out = (
        jnp.transpose(normal_out, (1, 0, 2))
        .reshape(tok_rows, heads_here * HEAD)
        .astype(jnp.bfloat16)
    )
    attn_heads = attn_query.shape[1] // HEAD
    key_heads = attn_key.shape[1] // HEAD
    group = attn_heads // key_heads
    joined = jnp.concatenate(
        [
            attn_key.reshape(tok_rows, key_heads, 1, HEAD),
            attn_value.reshape(tok_rows, key_heads, 1, HEAD),
        ],
        axis=2,
    ).reshape(tok_rows, key_heads * 2 * HEAD)
    padded = extended(joined, (("sp", 0),), WINDOW).reshape(-1, key_heads, 2, HEAD)
    offset = lax.axis_index("sp") * tok_rows
    total_rows = tok_rows * lax.axis_size("sp")
    head_ids = (lax.axis_index("tp") * attn_heads + jnp.arange(attn_heads)).astype(jnp.float32)
    slopes = jnp.exp2(-8.0 * (head_ids + 1.0) / ATTN_HEADS).reshape(key_heads, group, 1, 1)
    sink_logit = sink.reshape(key_heads, group, 1, 1)
    span = min(tok_rows, 512)
    pieces = []
    grouped = attn_query.reshape(span, key_heads, group, HEAD)
    scores = jnp.einsum(
        "qhge,khe->hgqk", grouped, padded[:, :, 0, :], preferred_element_type=jnp.float32
    ) * HEAD ** (-0.5)
    target = offset + 0 + jnp.arange(span, dtype=jnp.int32)
    source = offset + 0 - WINDOW + jnp.arange(span + 2 * WINDOW, dtype=jnp.int32)
    distance = jnp.abs(target[:, None] - source[None, :])
    valid = (distance <= WINDOW) & (source[None, :] >= 0) & (source[None, :] < total_rows)
    scores = jnp.where(valid, scores - slopes * distance.astype(jnp.float32), -jnp.inf)
    top = jnp.maximum(jnp.max(scores, axis=-1, keepdims=True), sink_logit)
    weights = jnp.exp(scores - top)
    probs = (
        weights / (jnp.sum(weights, axis=-1, keepdims=True) + jnp.exp(sink_logit - top))
    ).astype(jnp.bfloat16)
    result = jnp.einsum(
        "hgqk,khe->qhge", probs, padded[:, :, 1, :], preferred_element_type=jnp.float32
    )
    pieces.append(result.astype(jnp.bfloat16).reshape(span, attn_heads * HEAD))
    attn_out = pieces[0]
    return lax.psum_scatter(
        (
            jnp.dot(delta_out, delta_output_weight, preferred_element_type=jnp.float32)
            + jnp.dot(attn_out, attention_output_weight, preferred_element_type=jnp.float32)
        ).astype(jnp.bfloat16),
        "tp",
        scatter_dimension=0,
        tiled=True,
    )


def solution(mesh):
    in_specs = (
        P("sp", None),
        P(),
        P("sp", "tp"),
        P("sp", "tp"),
        P("sp", "tp"),
        P(),
        P(None, "tp"),
        P("tp", "sp"),
        P(None, "tp", None, None),
        P(),
        P("sp", "tp"),
        P("sp", "tp"),
        P("sp", "tp"),
        P("tp"),
        P("tp", None),
        P("tp", None),
    )
    out_specs = P(("sp", "tp"), None)
    return jax.shard_map(
        on_device, mesh=mesh, in_specs=in_specs, out_specs=out_specs, check_vma=False
    )
```

profile of v0, /device:TPU:0, one launch (start us, length us, event | category | flops | bytes accessed | tf_op | source)
XLA Modules:
  0.0 638.6 jit_solution(17557125246609413828)
XLA Ops:
  12.6 1.4 fusion.79
  16.1 57.2 %all-gather.8.cloned.1.call-done = bf16[2048,512]{1,0:T(8,128)(2,1)} async-done(((bf16[128,512]{1,0:T(8,128)(2,1)}), bf16[2048,512]{1,0:T(8,128)(2,1)}) %all-gather.8.cloned.1.call-update) | async-done | bytes 2097168 | tf_op jit(solution)/shard_map/all_gather | solution.py:167
  73.3 2.1 fusion.63
  84.4 1.4 fusion.131
  85.8 1.5 convolution_add_fusion.15
  87.3 47.9 %all-gather.10.cloned.1.call-done = bf16[2048,512]{1,0:T(8,128)(2,1)} async-done(((bf16[128,512]{1,0:T(8,128)(2,1)}), bf16[2048,512]{1,0:T(8,128)(2,1)}) %all-gather.10.cloned.1.call-update) | async-done | bytes 2097168 | tf_op jit(solution)/shard_map/all_gather | solution.py:168
  135.2 2.8 fusion.62
  140.3 2.1 copy.134
  142.6 2.0 convolution_add_fusion.14
  146.3 2.0 fusion.132
  149.4 6.9 %while.78 = (s32[]{:T(128)}, f32[8,64,64]{2,1,0:T(8,128)S(1)}, f32[8,64,64]{2,1,0:T(8,128)}, f32[2,8,64,64]{3,2,1,0:T(8,128)S(1)}, f32[2,8,64,64]{3,2,1,0:T(8,128)}, /*index=5*/s32[]{:T(128)}, s32[]{:T(128)}) while((s32[]{:T(128)}, f32[8,64,64]{2,1,0:T(8,128)S(1)}, f32[8,64,64]{2,1,0:T(8,128)}, f32[2,8,64,64]{3,2,1,0:T(8,128)S(1)}, ...), condition=%wide.region_4.5_spmd.clone, body=%wide.region_3.4_spmd.clone.sunk | while | flops 50397184 | bytes 2098267 | solution.py:92
  150.3 2.0 convolution_add_fusion.25
  153.8 2.1 convolution_add_fusion.25
  156.3 1.6 convert_bitcast_fusion.2
  157.9 2.1 reshape.323
  164.2 1.4 fusion.135
  165.7 1.5 convolution_add_fusion.12
  171.1 2.0 copy.140
  173.1 1.8 fusion.136
  174.9 2.0 convolution_add_fusion.11
  179.6 1.8 fusion.138
  183.6 6.9 %while.79 = (s32[]{:T(128)}, f32[8,64,64]{2,1,0:T(8,128)S(1)}, f32[8,64,64]{2,1,0:T(8,128)}, f32[2,8,64,64]{3,2,1,0:T(8,128)S(1)}, f32[2,8,64,64]{3,2,1,0:T(8,128)}, /*index=5*/s32[]{:T(128)}, s32[]{:T(128)}) while((s32[]{:T(128)}, f32[8,64,64]{2,1,0:T(8,128)S(1)}, f32[8,64,64]{2,1,0:T(8,128)}, f32[2,8,64,64]{3,2,1,0:T(8,128)S(1)}, ...), condition=%wide.region_7.8_spmd.clone, body=%wide.region_6.7_spmd.clone.sunk | while | flops 50397184 | bytes 2098267 | solution.py:92
  184.6 2.0 convolution_add_fusion.26
  188.1 2.0 convolution_add_fusion.26
  191.5 1.9 pad_maximum_fusion
  195.5 1.8 convolution_convert_fusion.6
  197.3 51.1 %all-gather.18.cloned.1.call-done = bf16[2048,256]{1,0:T(8,128)(2,1)} async-done(((bf16[128,256]{1,0:T(8,128)(2,1)}), bf16[2048,256]{1,0:T(8,128)(2,1)}) %all-gather.18.cloned.1.call-update) | async-done | bytes 1048592 | tf_op jit(solution)/shard_map/all_gather | solution.py:171
  248.5 1.7 convolution_convert_fusion.5
  251.0 3.3 collective-permute-start
  256.0 2.6 collective-permute-done
  258.6 3.5 collective-permute-done.1
  262.1 1.7 pad_maximum_fusion.1
  263.8 46.4 %all-gather.14.cloned.1.call-done = bf16[2048,512]{1,0:T(8,128)(2,1)} async-done(((bf16[128,512]{1,0:T(8,128)(2,1)}), bf16[2048,512]{1,0:T(8,128)(2,1)}) %all-gather.14.cloned.1.call-update) | async-done | bytes 2097168 | tf_op jit(solution)/shard_map/all_gather | solution.py:166
  310.3 3.0 fusion.61
  315.2 1.8 reverse.8
  317.0 1.7 broadcast_multiply_fusion
  318.7 2.1 reshape.329
  320.8 2.1 copy.153
  324.0 2.1 copy.147
  326.1 46.0 %all-gather.20.cloned.1.call-done = bf16[2048,512]{1,0:T(8,128)(2,1)} async-done(((bf16[128,512]{1,0:T(8,128)(2,1)}), bf16[2048,512]{1,0:T(8,128)(2,1)}) %all-gather.20.cloned.1.call-update) | async-done | bytes 2097168 | tf_op jit(solution)/shard_map/all_gather | solution.py:169
  372.1 2.9 convolution_convert_fusion.1
  375.0 1.7 copy.160
  376.7 1.6 fusion.126
  378.7 1.8 convolution_multiply_fusion
  380.5 1.8 convolution_multiply_fusion.1
  383.3 102.7 %all-gather.12.cloned.1.call-done = bf16[16,8,4,64,64]{4,3,2,1,0:T(8,128)(2,1)} async-done(((bf16[1,8,4,64,64]{4,3,2,1,0:T(8,128)(2,1)}), bf16[16,8,4,64,64]{4,3,2,1,0:T(8,128)(2,1)}) %all-gather.12.cloned.1.call-update) | async-done | bytes 4194320 | tf_op jit(solution)/shard_map/all_gather | solution.py:210
  486.0 11.3 %copy.142 = f32[16,8,4,64,64]{4,3,1,2,0:T(8,128)} copy(bf16[16,8,4,64,64]{4,3,2,1,0:T(8,128)(2,1)} %all-gather.12.cloned.1.call-done) | data formatting | bytes 12582912 | tf_op jit(solution)/shard_map/while | solution.py:226
  497.3 48.8 %while.76 = (s32[]{:T(128)}, f32[8,64,64]{2,1,0:T(8,128)S(1)}, s32[16]{0:T(128)S(1)}, s32[]{:T(128)}, f32[16,8,4,64,64]{4,3,1,2,0:T(8,128)}, /*index=5*/s32[]{:T(128)}, s32[]{:T(128)}) while((s32[]{:T(128)}, f32[8,64,64]{2,1,0:T(8,128)S(1)}, s32[16]{0:T(128)S(1)}, s32[]{:T(128)}, f32[16,8,4,64,64]{4,3,1,2,0:T(8,128)}, ...), condition=%wide.region_14.15_spmd, body=%wide.region_13.14_spmd.sunk | while | flops 25231364 | bytes 2490483 | solution.py:227
  546.9 11.4 %while.77 = (s32[]{:T(128)}, f32[8,64,64]{2,1,0:T(8,128)S(1)}, f32[2,8,64,64]{3,2,1,0:T(8,128)}, f32[2,8,64]{2,1,0:T(8,128)S(1)}, f32[2,8,64,64]{3,2,1,0:T(8,128...) while((s32[]{:T(128)}, f32[8,64,64]{2,1,0:T(8,128)S(1)}, ...), condition=%wide.region_16.17_spmd, body=%wide.region_15.16_spmd.sunk | while | flops 100827136 | bytes 3036333 | solution.py:124
  547.1 1.4 fusion.273
  548.5 1.4 convolution_subtract_fusion.7
  549.9 2.0 fusion.274
  552.8 1.4 fusion.273
  554.2 1.4 convolution_subtract_fusion.7
  555.7 2.0 fusion.274
  560.8 47.3 %while.74 = (s32[]{:T(128)}, f32[8,64,64]{2,1,0:T(8,128)S(1)}, s32[16]{0:T(128)S(1)}, s32[]{:T(128)}, f32[16,8,4,64,64]{4,3,1,2,0:T(8,128)}, /*index=5*/s32[]{:T(128)}) while((s32[]{:T(128)}, f32[8,64,64]{2,1,0:T(8,128)S(1)}, s32[16]{0:T(128)S(1)}, s32[]{:T(128)}, f32[16,8,4,64,64]{4,3,1,2,0:T(8,128)}, /*index=5*/s32[]{:T(128)}) %tuple.164), condition=%wide.region_9.10_spmd, body=%wide.region_8.9_spmd.sunk | while | flops 25231364 | bytes 2490463 | solution.py:226
  609.0 11.3 %while.75 = (s32[]{:T(128)}, f32[8,64,64]{2,1,0:T(8,128)S(1)}, f32[2,8,64,64]{3,2,1,0:T(8,128)}, f32[2,8,64]{2,1,0:T(8,128)S(1)}, f32[2,8,64,64]{3,2,1,0:T(8,128...) while((s32[]{:T(128)}, f32[8,64,64]{2,1,0:T(8,128)S(1)}, ...), condition=%wide.region_12.13_spmd, body=%wide.region_11.12_spmd.sunk | while | flops 100827136 | bytes 2905261 | solution.py:124
  609.2 1.4 fusion.261
  610.6 1.3 convolution_subtract_fusion.6
  612.0 2.1 fusion.262
  614.9 1.4 fusion.261
  616.3 1.3 convolution_subtract_fusion.6
  617.6 2.0 fusion.262
  625.1 6.3 reduce-scatter.2.cloned.1.call-done
  (341 shorter events, 137.6 us)
Async XLA Ops:
  6.5 616.7 %copy-start = (bf16[512,2048]{1,0:T(8,128)(2,1)S(1)}, bf16[512,2048]{1,0:T(8,128)(2,1)}, u32[]{:S(2)}) copy-start(bf16[512,2048]{1,0:T(8,128)(2,1)} %param.42) | copy-start | bytes 6291460
  6.5 66.7 %copy-start.14 = (bf16[128,2048]{1,0:T(8,128)(2,1)S(1)}, bf16[128,2048]{1,0:T(8,128)(2,1)}, u32[]{:S(2)}) copy-start(bf16[128,2048]{1,0:T(8,128)(2,1)} %param.28) | copy-start | bytes 1572868
  6.5 66.7 %copy-start.24 = (f32[2048]{0:T(1024)S(1)}, f32[2048]{0:T(1024)}, u32[]{:S(2)}) copy-start(f32[2048]{0:T(1024)} %param.29) | copy-start | bytes 24580
  6.5 7.5 %copy-start.25 = (f32[8,128]{1,0:T(8,128)S(1)}, f32[8,128]{1,0:T(8,128)}, u32[]{:S(2)}) copy-start(f32[8,128]{1,0:T(8,128)} %param.35) | copy-start | bytes 12292
  6.5 66.7 %all-gather.8.cloned.1.call-start = ((), (), s32[]{:S(2)}) async-start(), calls=%async_computation.1 | async-start | bytes 2228224 | tf_op jit(solution)/shard_map/all_gather | solution.py:167
  7.3 128.0 %all-gather.10.cloned.1.call-start = ((), (), s32[]{:S(2)}) async-start(), calls=%async_computation.2 | async-start | bytes 2228224 | tf_op jit(solution)/shard_map/all_gather | solution.py:168
  8.0 187.4 %all-gather.16.cloned.1.call-start = ((), (), s32[]{:S(2)}) async-start(), calls=%async_computation.5 | async-start | bytes 1114112 | tf_op jit(solution)/shard_map/all_gather | solution.py:170
  8.8 239.7 %all-gather.18.cloned.1.call-start = ((), (), s32[]{:S(2)}) async-start(), calls=%async_computation.6 | async-start | bytes 1114112 | tf_op jit(solution)/shard_map/all_gather | solution.py:171
  9.3 300.9 %all-gather.14.cloned.1.call-start = ((), (), s32[]{:S(2)}) async-start(), calls=%async_computation.4 | async-start | bytes 2228224 | tf_op jit(solution)/shard_map/all_gather | solution.py:166
  9.9 362.2 %all-gather.20.cloned.1.call-start = ((), (), s32[]{:S(2)}) async-start(), calls=%async_computation.7 | async-start | bytes 2228224 | tf_op jit(solution)/shard_map/all_gather | solution.py:169
  10.5 475.5 %all-gather.12.cloned.1.call-start = ((), (), s32[]{:S(2)}) async-start(), calls=%async_computation.3 | async-start | bytes 8912896 | tf_op jit(solution)/shard_map/all_gather | solution.py:210
  138.0 4.6 copy-start.16
  139.2 5.5 copy-start.15
  142.4 2.3 copy-start.18
  142.6 5.7 copy-start.3
  145.4 3.9 copy-start.7
  146.3 3.0 copy-start.10
  161.2 20.3 %copy-start.1 = (f32[8,2,64,64]{3,2,0,1:T(8,128)}, f32[8,2,64,64]{3,2,0,1:T(8,128)S(1)}, u32[]{:S(2)}) copy-start(f32[8,2,64,64]{3,2,0,1:T(8,128)S(1)} %copy.137) | copy-start | bytes 786436
  176.9 2.0 copy-start.17
  177.6 2.0 copy-start.5
  179.6 4.0 copy-start.9
  182.4 1.3 copy-start.11
  193.5 437.9 %reduce-scatter.2.cloned.1.call-start = ((), (), s32[]{:S(2)}) async-start(), calls=%async_computation.8 | async-start | bytes 786432 | tf_op jit(solution)/shard_map/reduce_scatter | solution.py:278
  195.4 60.5 %copy-start.27 = (f32[8]{0:T(128)S(1)}, f32[8]{0:T(128)}, u32[]{:S(2)}) copy-start(f32[8]{0:T(128)} %param.41) | copy-start | bytes 100
  251.0 7.6 %collective-permute-start = (bf16[128,512]{0,1:T(8,128)(2,1)}, bf16[128,512]{0,1:T(8,128)(2,1)S(1)}, u32[]{:S(2)}, u32[]{:S(2)}) collective-permute-start(bf16[128,512]{0,1:T(8,128)(2,1)} %bitcast.71), channel_id=1, source_target_pairs={{0,2},{2,4},{4,6},{6,8},{8,10},{10,12},{12,14},{14,16},{16,18},{18... | collective-permute-start | bytes 393224 | tf_op jit(solution)/shard_map/ppermute | solution.py:20
  254.4 7.7 %collective-permute-start.1 = (bf16[128,512]{0,1:T(8,128)(2,1)}, bf16[128,512]{0,1:T(8,128)(2,1)}, u32[]{:S(2)}, u32[]{:S(2)}) collective-permute-start(bf16[128,512]{0,1:T(8,128)(2,1)} %bitcast.71), channel_id=1, source_target_pairs={{2,0},{4,2},{6,4},{8,6},{10,8},{12,10},{14,12},{16,14},{18,16},{20... | collective-permute-start | bytes 393224 | tf_op jit(solution)/shard_map/ppermute | solution.py:23
  315.2 7.7 %copy-start.20 = (f32[8,128,64]{1,2,0:T(8,128)S(1)}, f32[8,128,64]{1,2,0:T(8,128)}, u32[]{:S(2)}) copy-start(f32[8,128,64]{1,2,0:T(8,128)} %get-tuple-element.499) | copy-start | bytes 786436
  324.0 52.7 %copy-start.22 = (f32[128,384]{0,1:T(8,128)S(1)}, f32[128,384]{0,1:T(8,128)}, u32[]{:S(2)}) copy-start(f32[128,384]{0,1:T(8,128)} %fusion.93) | copy-start | bytes 589828
  376.7 2.0 copy-start.2
  376.7 2.0 copy-start.13
  378.3 2.2 copy-start.12
  378.4 3.9 copy-start.21
  497.3 49.6 %copy-start.6 = (f32[2,8,64,64]{3,2,1,0:T(8,128)S(1)}, f32[2,8,64,64]{3,2,1,0:T(8,128)}, u32[]{:S(2)}) copy-start(f32[2,8,64,64]{3,2,1,0:T(8,128)} %bitcast_multiply_fusion.6) | copy-start | bytes 786436
  560.8 48.2 %copy-start.4 = (f32[2,8,64,64]{3,2,1,0:T(8,128)S(1)}, f32[2,8,64,64]{3,2,1,0:T(8,128)}, u32[]{:S(2)}) copy-start(f32[2,8,64,64]{3,2,1,0:T(8,128)} %copy-done.3) | copy-start | bytes 786436
  560.8 48.2 %copy-start.8 = (f32[2,8,64,64]{3,2,1,0:T(8,128)S(1)}, f32[2,8,64,64]{3,2,1,0:T(8,128)}, u32[]{:S(2)}) copy-start(f32[2,8,64,64]{3,2,1,0:T(8,128)} %copy-done.7) | copy-start | bytes 786436
  620.3 2.8 copy-start.26
  622.0 1.8 copy-start.19
  622.0 1.8 copy-start.23
Sparse Core Ops, SparseCore 0:
  10.1 63.0 all-gather.7
  76.0 59.1 all-gather.9
  138.0 53.8 all-gather.15
  194.5 53.9 all-gather.17
  251.1 59.1 all-gather.13
  312.9 59.1 all-gather.19
  374.9 111.0 all-gather.11
  625.2 6.0 reduce-scatter.1
where the time goes:
time: 651 us; the launch traced here: 639 us
  waiting for transfers between devices  367 us (56%)
  local copies, waits for them, and re-layouts  114 us (18%)
  matrix products  99.6 us (15%)
  loops' own time  21.4 us (3%)
  other arithmetic  16.7 us (3%)
  between operations  14.7 us (2%)
    all_gather x1, waiting for transfers between devices, on_device(): lax.all_gather(stacked.astype(jnp.bfloat16), 'sp', axis=0, tiled=True)  103 us
    dot_general x88, matrix products, outer_product(): return jnp.einsum(spec, left, right, precision=lax.Precision.HIGHEST)  79.6 us
    all_gather x1, waiting for transfers between devices, on_device(): lax.all_gather(delta_key_weight, 'sp', axis=0, tiled=True)  57.2 us
    all_gather x1, waiting for transfers between devices, on_device(): lax.all_gather(attention_value_weight, 'sp', axis=0, tiled=True)  51.1 us
    all_gather x1, waiting for transfers between devices, on_device(): lax.all_gather(delta_value_weight, 'sp', axis=0, tiled=True)  47.9 us
    all_gather x1, waiting for transfers between devices, on_device(): lax.all_gather(delta_query_weight, 'sp', axis=0, tiled=True)  46.4 us
    all_gather x1, waiting for transfers between devices, on_device(): lax.all_gather(attention_query_weight, 'sp', axis=0, tiled=True)  46 us
    squeeze x32, local copies, waits for them, and re-layouts, on_device(): lax.scan(forward_apply, starting_state[0], (places, every))  42.6 us
  transfers between devices with their start and end apart: 10, of which 9 were waited for; matrix products, arithmetic and copies ran while one was open for 18% of the time, Pallas kernels for 0%

commit v1 on v0

v1 whole, which is shorter than its diff:
```python
import functools

import jax
import jax.numpy as jnp
from jax import lax
from jax.experimental import pallas as pl
from jax.experimental.pallas import tpu as pltpu
from jax.sharding import PartitionSpec as P

HEAD = 64
WINDOW = 128
EPS = 1e-06
F32 = jnp.float32
BF16 = jnp.bfloat16


def ring_dims(mesh):
    names = list(mesh.axis_names)
    count = mesh.shape["sp"]
    devices = mesh.devices
    at = names.index("sp")
    line = [devices[tuple(i if k == at else 0 for k in range(len(names)))] for i in range(count)]
    try:
        coords = [tuple(d.coords) for d in line]
        dims = []
        for axis in range(len(coords[0])):
            size = len({c[axis] for c in coords})
            if size > 1:
                first = coords[0][axis]
                stride = next(i for i in range(count) if coords[i][axis] != first)
                dims.append((size, stride))
        dims.sort(key=lambda d: -d[1])
        total = 1
        for size, stride in reversed(dims):
            if stride != total:
                return ((count, 1),)
            total *= size
        return tuple(dims) if total == count else ((count, 1),)
    except Exception:
        return ((count, 1),)


def tree(dims, order, lean):
    zero = (0,) * len(dims)
    nodes, level = [], [zero]
    held = [zero]
    for d in order:
        size = dims[d][0]
        up = size // 2 if lean else (size - 1) // 2
        down = size - 1 - up
        for far in range(1, max(up, down) + 1):
            for base in held:
                for step, reach in ((1, up), (-1, down)):
                    if far <= reach:
                        here, parent = list(base), list(base)
                        here[d] = (step * far) % size
                        parent[d] = (step * (far - 1)) % size
                        nodes.append((tuple(here), tuple(parent), d, step))
        held = [b[:d] + (r,) + b[d + 1 :] for b in held for r in range(size)]
    return nodes


def piece_trees(dims, pieces):
    count = len(dims)
    fore = list(range(count))
    orders = [fore, fore[:1] + fore[1:][::-1], fore[1:] + fore[:1], fore[1:][::-1] + fore[:1]]
    return [tree(dims, orders[p % 4], p % 2 == 0) for p in range(pieces)]


def dot(left, right, dims=((1,), (0,))):
    return lax.dot_general(
        left.astype(BF16), right.astype(BF16), (dims, ((), ())), preferred_element_type=F32
    )


def exact_dot(left, right, dims):
    return lax.dot_general(
        left, right, (dims, ((), ())), precision=lax.Precision.HIGHEST, preferred_element_type=F32
    )


def kernel(
    cfg,
    tokens_ref,
    gain_ref,
    gate_ref,
    params_ref,
    increments_ref,
    start_ref,
    norm_gain_ref,
    logits_ref,
    wd_ref,
    wa_ref,
    delta_out_hbm,
    attn_out_hbm,
    out_ref,
    norm3,
    dbuf,
    abuf,
    dacc,
    aacc,
    proj,
    aq,
    kv,
    halo,
    mine,
    maps,
    state,
    base_out,
    reads,
    feats,
    wo,
    partial,
    prec,
    d_send,
    d_recv,
    a_send,
    a_recv,
    m_send,
    m_recv,
    h_send,
    h_recv,
    p_send,
    p_recv,
    w_sem,
):
    n, ntp, dims, heads, attn_heads, key_heads = cfg
    me, mt = lax.axis_index("sp"), lax.axis_index("tp")
    rows, width = tokens_ref.shape
    kd = width // n
    dcols, acols = heads * HEAD, attn_heads * HEAD
    kcols = key_heads * HEAD

    barrier = pltpu.get_barrier_semaphore()
    for k in range(1, n):
        pl.semaphore_signal(barrier, inc=1, device_id={"sp": lax.rem(me + k, n)})
    for k in range(1, ntp):
        pl.semaphore_signal(barrier, inc=1, device_id={"tp": lax.rem(mt + k, ntp)})
    pl.semaphore_wait(barrier, n - 1 + ntp - 1)

    def shifted(d, step):
        size, stride = dims[d]
        digit = lax.rem(me // stride, size)
        return me + (lax.rem(digit + step + size, size) - digit) * stride

    def slot(offset):
        at = 0
        for (size, stride), o in zip(dims, offset):
            at = at + o * stride
        return at

    def source(offset):
        at = 0
        for (size, stride), o in zip(dims, offset):
            digit = lax.rem(me // stride, size)
            at = at + lax.rem(digit - o + size, size) * stride
        return at

    def gather(own, buf, send, recv):
        trees = piece_trees(dims, buf.shape[0])
        started = []

        def copy(p, node):
            here, parent, d, step = node
            a, b = slot(parent), slot(here)
            return pltpu.make_async_remote_copy(
                src_ref=own.at[p] if a == 0 else buf.at[p, a],
                dst_ref=buf.at[p, b],
                send_sem=send.at[p, b],
                recv_sem=recv.at[p, b],
                device_id={"sp": shifted(d, step)},
            )

        def forward(p, offset):
            for node in trees[p]:
                if node[1] == offset:
                    made = copy(p, node)
                    made.start()
                    started.append(made)

        def begin():
            for p in range(len(trees)):
                forward(p, (0,) * len(dims))

        def arrive(index, acc):
            for p in range(len(trees)):
                copy(p, trees[p][index]).wait_recv()
                forward(p, trees[p][index][0])
            for p in range(len(trees)):
                here = trees[p][index][0]
                acc[p] += dot(norm3[source(here)], buf[p, slot(here)])

        return begin, arrive, started

    d_begin, d_arrive, d_started = gather(wd_ref, dbuf, d_send, d_recv)
    a_begin, a_arrive, a_started = gather(wa_ref, abuf, a_send, a_recv)
    d_begin()
    w_copies = [
        pltpu.make_async_copy(delta_out_hbm, wo.at[0], w_sem.at[0]),
        pltpu.make_async_copy(attn_out_hbm, wo.at[1], w_sem.at[1]),
    ]
    for made in w_copies:
        made.start()

    wide = tokens_ref[...].astype(F32)
    normed = (
        wide * lax.rsqrt(jnp.mean(wide * wide, axis=-1, keepdims=True) + EPS) * gain_ref[...]
    ).astype(BF16)
    for j in range(n):
        norm3[j] = normed[:, j * kd : (j + 1) * kd]
    gates = dot(gate_ref[...], normed, ((1,), (1,)))
    rates = jnp.exp(params_ref[:, 0:1])
    offsets = params_ref[:, 1:2]
    row = lax.broadcasted_iota(jnp.int32, (rows, rows), 0)
    col = lax.broadcasted_iota(jnp.int32, (rows, rows), 1)
    eye = (row == col).astype(F32)
    sums_row, sums_col, strength_col = [], [], []
    for r in range(2):
        x = gates[r * heads : (r + 1) * heads]
        soft = jnp.maximum(x, 0.0) + jnp.log1p(jnp.exp(-jnp.abs(x)))
        decay = increments_ref[...] - rates * soft
        y = gates[(2 + r) * heads : (3 + r) * heads] + offsets
        strength = 1.0 / (1.0 + jnp.exp(-y))
        tri = ((row >= col) if r == 0 else (row <= col)).astype(F32)
        sums_row.append(exact_dot(decay, tri, ((1,), (1,))))
        sums_col.append(exact_dot(tri, decay, ((1,), (1,))))
        strength_col.append(exact_dot(eye, strength, ((1,), (1,))))
    for p in range(wd_ref.shape[0]):
        dacc[p] = dot(norm3[me], wd_ref[p])
    for p in range(wa_ref.shape[0]):
        aacc[p] = dot(norm3[me], wa_ref[p])
    for index in range(n - 1):
        d_arrive(index, dacc)
    a_begin()
    per = dacc.shape[2]
    for p in range(dacc.shape[0]):
        proj[:, p * per : (p + 1) * per] = dacc[p].astype(BF16)

    lane = lax.broadcasted_iota(jnp.int32, (HEAD, 2 * HEAD), 1)
    sub = lax.broadcasted_iota(jnp.int32, (HEAD, 2 * HEAD), 0)
    turn = jnp.where(lane < HEAD, 1.0, -1.0)
    shift_eye = (lane == sub + HEAD).astype(F32)
    same = {s: (row // s) == (col // s) for s in (16, 32, 64, 128)}

    def delta_group(some):
        chains = []
        for h in some:
            q = proj[:, h * HEAD : (h + 1) * HEAD].astype(F32)
            k = proj[:, dcols + h * HEAD : dcols + (h + 1) * HEAD].astype(F32)
            v = proj[:, 2 * dcols + h * HEAD : 2 * dcols + (h + 1) * HEAD].astype(F32)
            q = q * (lax.rsqrt(jnp.sum(q * q, axis=-1, keepdims=True) + EPS) * HEAD ** (-0.5))
            k = k * lax.rsqrt(jnp.sum(k * k, axis=-1, keepdims=True) + EPS)
            gram = dot(k, k, ((1,), (1,)))
            cross = dot(q, k, ((1,), (1,)))
            for r in range(2):
                incl = (row >= col) if r == 0 else (row <= col)
                c_row = sums_row[r][h : h + 1, :]
                c_col = sums_col[r][:, h : h + 1]
                b_col = strength_col[r][:, h : h + 1]
                total = c_col[rows - 1 : rows] if r == 0 else c_col[0:1]
                w = jnp.exp(jnp.where(incl, c_col - c_row, -1e30))
                low = jnp.where(row == col, 0.0, gram * w) * b_col
                grown = jnp.exp(c_col)
                rhs = jnp.concatenate([v * b_col, k * (b_col * grown)], axis=1)
                chains.append(
                    dict(
                        h=h,
                        r=r,
                        low=low,
                        rhs=rhs,
                        mix=cross * w,
                        carried=k * jnp.exp(total - c_col),
                        q=q * grown,
                        total=total,
                    )
                )
        for c in chains:
            base = jnp.where(same[16], c["low"], 0.0)
            c["inv"], c["pow"] = eye - base, base
        for _ in range(3):
            for c in chains:
                c["pow"] = dot(c["pow"], c["pow"])
            for c in chains:
                c["inv"] = c["inv"] + dot(c["inv"], c["pow"])
        for s in (32, 64, 128):
            for c in chains:
                off = jnp.where(same[s] & jnp.logical_not(same[s // 2]), c["low"], 0.0)
                c["tmp"] = dot(off, c["inv"])
            for c in chains:
                c["inv"] = c["inv"] - dot(c["inv"], c["tmp"])
        for c in chains:
            c["uw"] = dot(c["inv"], c["rhs"])
        for c in chains:
            mapped = dot(c["carried"], c["uw"], ((0,), (0,))) * turn
            mapped = mapped + shift_eye * jnp.exp(c["total"])
            mine[c["r"], c["h"]] = mapped.astype(BF16)
            c["read"] = dot(c["mix"], c["uw"])
        for f, b in zip(chains[::2], chains[1::2]):
            base_out[f["h"]] = f["read"][:, :HEAD] + b["read"][:, :HEAD]
            reads[f["h"]] = jnp.concatenate(
                [f["q"] - f["read"][:, HEAD:], b["q"] - b["read"][:, HEAD:]], axis=1
            ).astype(BF16)

    batch = min(2, heads)
    groups = heads // batch
    done = 0
    for g in range(groups):
        delta_group(range(g * batch, (g + 1) * batch))
        upto = (n - 1) * (g + 1) // groups if g < groups - 1 else done
        while done < upto:
            a_arrive(done, aacc)
            done += 1

    m_copies = []
    for k in range(1, n):
        made = pltpu.make_async_remote_copy(
            src_ref=mine.at[(me + k) // n],
            dst_ref=maps.at[me],
            send_sem=m_send.at[k],
            recv_sem=m_recv.at[me],
            device_id={"sp": lax.rem(me + k, n)},
        )
        made.start()
        m_copies.append(made)

    while done < n - 1:
        a_arrive(done, aacc)
        done += 1
    per_a = aacc.shape[2]
    for p in range(aacc.shape[0]):
        prec[:, p * per_a : (p + 1) * per_a] = aacc[p].astype(BF16)
    kv[...] = prec[:, acols : acols + 2 * kcols]
    h_copies = []
    for at, step in ((0, 1), (1, n - 1)):
        made = pltpu.make_async_remote_copy(
            src_ref=kv,
            dst_ref=halo.at[at],
            send_sem=h_send.at[at],
            recv_sem=h_recv.at[at],
            device_id={"sp": lax.rem(me + step, n)},
        )
        made.start()
        h_copies.append(made)
    for made in h_copies:
        made.wait_recv()

    gap = (row - col).astype(F32)
    far_low, far_high = gap + rows, rows - gap
    ok_low = (far_low <= WINDOW) & (me > 0)
    ok_high = (far_high <= WINDOW) & (me < n - 1)
    bias = [
        jnp.where(ok_low, far_low, 1e30),
        jnp.where(jnp.abs(gap) <= WINDOW, jnp.abs(gap), 1e30),
        jnp.where(ok_high, far_high, 1e30),
    ]
    share = attn_heads // key_heads
    for h in range(attn_heads):
        at = (h // share) * HEAD
        q = prec[:, h * HEAD : (h + 1) * HEAD]
        slope = logits_ref[h : h + 1, 0:1]
        sink = logits_ref[h : h + 1, 1:2]
        parts = [halo.at[0], kv, halo.at[1]]
        keys = [part[:, at : at + HEAD] for part in parts]
        vals = [part[:, kcols + at : kcols + at + HEAD] for part in parts]
        scores = [
            dot(q, k, ((1,), (1,))) * HEAD ** (-0.5) - slope * b for k, b in zip(keys, bias)
        ]
        top = jnp.maximum(jnp.maximum(scores[0], scores[1]), scores[2])
        top = jnp.maximum(jnp.max(top, axis=-1, keepdims=True), sink)
        weights = [jnp.exp(s - top) for s in scores]
        total = jnp.sum(weights[0] + weights[1] + weights[2], axis=-1, keepdims=True)
        scale = 1.0 / (total + jnp.exp(sink - top))
        res = dot(weights[0], vals[0]) + dot(weights[1], vals[1]) + dot(weights[2], vals[2])
        feats[:, dcols + h * HEAD : dcols + (h + 1) * HEAD] = (res * scale).astype(BF16)

    state[...] = start_ref[...]

    def apply(r, s):
        pltpu.make_async_remote_copy(
            src_ref=mine.at[0],
            dst_ref=maps.at[s],
            send_sem=m_send.at[0],
            recv_sem=m_recv.at[s],
            device_id={"sp": lax.rem(me + 1, n)},
        ).wait_recv()
        for h in range(heads):
            m = maps[s, h]
            now = state[r, h]
            high = now.astype(BF16)
            rest = (now - high.astype(F32)).astype(BF16)
            moved = dot(m[:, HEAD:], jnp.concatenate([high, rest], axis=1))
            state[r, h] = moved[:, :HEAD] + moved[:, HEAD:] + m[:, :HEAD].astype(F32)

    def forward_step(i, carry):
        apply(0, i)
        return carry

    def backward_step(i, carry):
        apply(1, n - 1 - i)
        return carry

    lax.fori_loop(0, me, forward_step, 0)
    lax.fori_loop(0, n - 1 - me, backward_step, 0)

    for h in range(heads):
        both = jnp.concatenate([state[0, h], state[1, h]], axis=0)
        y = base_out[h] + dot(reads[h], both)
        y = y * lax.rsqrt(jnp.mean(y * y, axis=-1, keepdims=True) + EPS) * norm_gain_ref[...]
        feats[:, h * HEAD : (h + 1) * HEAD] = y.astype(BF16)

    for made in w_copies:
        made.wait()
    step = min(512, width)
    each = rows // ntp
    for at in range(0, width, step):
        res = dot(feats[:, :dcols], wo[0, :, at : at + step]) + dot(
            feats[:, dcols:], wo[1, :, at : at + step]
        )
        res = res.astype(BF16)
        for p in range(ntp):
            partial[0, p, :, at : at + step] = res[p * each : (p + 1) * each]
    p_copies = []
    for k in range(1, ntp):
        peer = lax.rem(mt + k, ntp)
        made = pltpu.make_async_remote_copy(
            src_ref=partial.at[0, peer],
            dst_ref=partial.at[1, k],
            send_sem=p_send.at[k],
            recv_sem=p_recv.at[k],
            device_id={"tp": peer},
        )
        made.start()
        p_copies.append(made)
    total = partial[0, mt].astype(F32)
    for k in range(1, ntp):
        p_copies[k - 1].wait_recv()
        total = total + partial[1, k].astype(F32)
    out_ref[...] = total.astype(BF16)
    for made in d_started + a_started + m_copies + h_copies + p_copies:
        made.wait_send()


def cut(weights):
    joined = jnp.concatenate(weights, axis=1)
    rows, cols = joined.shape
    pieces = 4 if cols % 512 == 0 else 1
    return jnp.transpose(joined.reshape(rows, pieces, cols // pieces), (1, 0, 2))


def on_device(
    dims,
    tokens,
    input_norm_gain,
    delta_query_weight,
    delta_key_weight,
    delta_value_weight,
    gate_weight,
    head_decay_params,
    log_decay_increments,
    starting_state,
    delta_norm_gain,
    attention_query_weight,
    attention_key_weight,
    attention_value_weight,
    sink,
    delta_output_weight,
    attention_output_weight,
):
    n, ntp = lax.axis_size("sp"), lax.axis_size("tp")
    rows, width = tokens.shape
    heads = delta_query_weight.shape[1] // HEAD
    attn_heads = attention_query_weight.shape[1] // HEAD
    key_heads = attention_key_weight.shape[1] // HEAD
    gates = lax.dynamic_slice_in_dim(gate_weight, lax.axis_index("tp") * heads, heads, 2)
    gates = gates.reshape(gate_weight.shape[0], 4 * heads).T
    wd = cut([delta_query_weight, delta_key_weight, delta_value_weight])
    wa = cut([attention_query_weight, attention_key_weight, attention_value_weight])
    head_ids = (lax.axis_index("tp") * attn_heads + jnp.arange(attn_heads)).astype(F32)
    slopes = jnp.exp2(-8.0 * (head_ids + 1.0) / (attn_heads * ntp))
    logits = jnp.stack([slopes, sink], axis=1)
    cfg = (n, ntp, dims, heads, attn_heads, key_heads)
    dcols, acols, kcols = heads * HEAD, attn_heads * HEAD, key_heads * HEAD
    pd, pa = wd.shape[0], wa.shape[0]
    vmem = pl.BlockSpec(memory_space=pltpu.VMEM)
    hbm = pl.BlockSpec(memory_space=pl.ANY)
    dma = pltpu.SemaphoreType.DMA
    return pl.pallas_call(
        functools.partial(kernel, cfg),
        out_shape=jax.ShapeDtypeStruct((rows // ntp, width), BF16),
        in_specs=[vmem] * 10 + [hbm] * 2,
        out_specs=vmem,
        scratch_shapes=[
            pltpu.VMEM((n, rows, width // n), BF16),
            pltpu.VMEM((pd, n) + wd.shape[1:], BF16),
            pltpu.VMEM((pa, n) + wa.shape[1:], BF16),
            pltpu.VMEM((pd, rows, wd.shape[2]), F32),
            pltpu.VMEM((pa, rows, wa.shape[2]), F32),
            pltpu.VMEM((rows, 3 * dcols), BF16),
            pltpu.VMEM((8, 128), BF16),
            pltpu.VMEM((rows, 2 * kcols), BF16),
            pltpu.VMEM((2, rows, 2 * kcols), BF16),
            pltpu.VMEM((2, heads, HEAD, 2 * HEAD), BF16),
            pltpu.VMEM((n, heads, HEAD, 2 * HEAD), BF16),
            pltpu.VMEM((2, heads, HEAD, HEAD), F32),
            pltpu.VMEM((heads, rows, HEAD), F32),
            pltpu.VMEM((heads, rows, 2 * HEAD), BF16),
            pltpu.VMEM((rows, dcols + acols), BF16),
            pltpu.VMEM((2,) + delta_output_weight.shape, BF16),
            pltpu.VMEM((2, ntp, rows // ntp, width), BF16),
            pltpu.VMEM((rows, acols + 2 * kcols), BF16),
            dma((pd, n)),
            dma((pd, n)),
            dma((pa, n)),
            dma((pa, n)),
            dma((n,)),
            dma((n,)),
            dma((2,)),
            dma((2,)),
            dma((ntp,)),
            dma((ntp,)),
            dma((2,)),
        ],
        compiler_params=pltpu.CompilerParams(
            collective_id=0, has_side_effects=True, vmem_limit_bytes=60 * 1024 * 1024
        ),
    )(
        tokens,
        input_norm_gain.reshape(1, -1),
        gates,
        head_decay_params.T,
        log_decay_increments,
        starting_state,
        delta_norm_gain.reshape(1, -1),
        logits,
        wd,
        wa,
        delta_output_weight,
        attention_output_weight,
    )


def solution(mesh):
    in_specs = (
        P("sp", None),
        P(),
        P("sp", "tp"),
        P("sp", "tp"),
        P("sp", "tp"),
        P(),
        P(None, "tp"),
        P("tp", "sp"),
        P(None, "tp", None, None),
        P(),
        P("sp", "tp"),
        P("sp", "tp"),
        P("sp", "tp"),
        P("tp"),
        P("tp", None),
        P("tp", None),
    )
    out_specs = P(("sp", "tp"), None)
    return jax.shard_map(
        functools.partial(on_device, ring_dims(mesh)),
        mesh=mesh,
        in_specs=in_specs,
        out_specs=out_specs,
        check_vma=False,
    )
```

time: 651 us -> 189 us (0.29)
  the two profiles are of different devices: /device:TPU:0 before, /device:TPU:15 now
where the time goes in v1:
time: 189 us
  Pallas kernels  176 us (93%)
  local copies, waits for them, and re-layouts  11.2 us (6%)
    pallas_call x1, Pallas kernels, on_device(): pl.pallas_call(functools.partial(kernel, cfg), out_shape=jax.ShapeDtypeSt...  176 us
    unnamed x12, local copies, waits for them, and re-layouts  8.11 us

profile of v1, /device:TPU:15, one launch (start us, length us, event | category | flops | bytes accessed | tf_op | source)
XLA Modules:
  0.0 188.5 jit_solution(17810799266198772639)
XLA Ops:
  0.0 0.0 copy-start
  0.0 0.0 copy-start.1
  0.0 0.7 pad_maximum_fusion.2
  0.7 0.7 copy.38.logits_ref
  1.4 1.3 copy.29
  2.7 0.9 copy.35
  3.7 1.0 copy.36
  4.7 0.0 copy-done
  4.7 0.7 dynamic-slice_bitcast_fusion.gate_ref
  5.3 1.0 copy.30
  6.4 1.0 copy.31
  7.4 1.0 copy.32
  8.5 0.9 copy.33
  9.4 0.0 copy-done.1
  9.4 0.1 copy.34
  9.5 0.9 copy.37
  10.4 176.4 %shard_map.154 = bf16[64,2048]{1,0:T(8,128)(2,1)} custom-call(bf16[128,2048]{1,0:T(8,128)(2,1)} %tokens_ref.1, f32[1,2048]{1,0:T(1,128)} %bitcast.17, bf16[32,2048]{1,0:T(8,128)(2,1)} %dynamic-slice_bitcast_fusion.gate_ref, f32[8,2]{1,0:T(8,128)} %bitcast.16, f32[8,128]{1,0:T(8,128)} %increments_ref.1, f32[2,8,64,64]{3,2,1,0:T(8,128)} %start_ref.1, ...), custom_call_target="tpu_custom_call" | custom-call | tf_op jit(solution)/shard_map/pallas_call | solution.py:487
  186.8 1.7 copy.40
  (3 shorter events, 0.1 us)
Async XLA Ops:
  0.0 4.7 %copy-start = (bf16[2048,4,16]{0,2,1:T(8,128)(2,1)S(1)}, bf16[2048,4,16]{0,2,1:T(8,128)(2,1)}, u32[]{:S(2)}) copy-start(bf16[2048,4,16]{0,2,1:T(8,128)(2,1)} %param.21) | copy-start | bytes 786436
  0.0 9.4 %copy-start.1 = (bf16[128,512]{1,0:T(8,128)(2,1)S(1)}, bf16[128,512]{1,0:T(8,128)(2,1)}, u32[]{:S(2)}) copy-start(bf16[128,512]{1,0:T(8,128)(2,1)} %param.26) | copy-start | bytes 393220

commit v2 on v1

--- a/solution.py
+++ b/solution.py
@@ -40,31 +40,25 @@
         return ((count, 1),)
 
 
-def tree(dims, order, lean):
-    zero = (0,) * len(dims)
-    nodes, level = [], [zero]
-    held = [zero]
+def piece_orders(dims, pieces):
+    count = len(dims)
+    if count == 3:
+        orders = [(2, 0, 1), (1, 0, 2)]
+    elif count == 2:
+        orders = [(0, 1), (1, 0)]
+    else:
+        orders = [tuple(range(count))]
+    return [orders[p % len(orders)] for p in range(pieces)]
+
+
+def arrivals(dims, order):
+    held, nodes = [(0,) * len(dims)], []
     for d in order:
         size = dims[d][0]
-        up = size // 2 if lean else (size - 1) // 2
-        down = size - 1 - up
-        for far in range(1, max(up, down) + 1):
-            for base in held:
-                for step, reach in ((1, up), (-1, down)):
-                    if far <= reach:
-                        here, parent = list(base), list(base)
-                        here[d] = (step * far) % size
-                        parent[d] = (step * (far - 1)) % size
-                        nodes.append((tuple(here), tuple(parent), d, step))
+        turns = sorted(range(1, size), key=lambda r: (min(r, size - r), r))
+        nodes += [(b[:d] + (r,) + b[d + 1 :], d) for r in turns for b in held]
         held = [b[:d] + (r,) + b[d + 1 :] for b in held for r in range(size)]
     return nodes
-
-
-def piece_trees(dims, pieces):
-    count = len(dims)
-    fore = list(range(count))
-    orders = [fore, fore[:1] + fore[1:][::-1], fore[1:] + fore[:1], fore[1:][::-1] + fore[:1]]
-    return [tree(dims, orders[p % 4], p % 2 == 0) for p in range(pieces)]
 
 
 def dot(left, right, dims=((1,), (0,))):
@@ -89,45 +83,50 @@
     start_ref,
     norm_gain_ref,
     logits_ref,
-    wd_ref,
-    wa_ref,
-    delta_out_hbm,
-    attn_out_hbm,
-    out_ref,
-    norm3,
-    dbuf,
-    abuf,
-    dacc,
-    aacc,
-    proj,
-    aq,
-    kv,
-    halo,
-    mine,
-    maps,
-    state,
-    base_out,
-    reads,
-    feats,
-    wo,
-    partial,
-    prec,
-    d_send,
-    d_recv,
-    a_send,
-    a_recv,
-    m_send,
-    m_recv,
-    h_send,
-    h_recv,
-    p_send,
-    p_recv,
-    w_sem,
+    *refs,
 ):
-    n, ntp, dims, heads, attn_heads, key_heads = cfg
+    parts = cfg[-2:]
+    count = parts[0] + parts[1]
+    w_refs, refs = refs[:count], refs[count:]
+    (
+        delta_out_hbm,
+        attn_out_hbm,
+        out_ref,
+        norm3,
+        dbuf,
+        abuf,
+        dacc,
+        aacc,
+        proj,
+        aq,
+        kv,
+        halo,
+        mine,
+        maps,
+        state,
+        base_out,
+        reads,
+        feats,
+        wo,
+        partial,
+        prec,
+        d_send,
+        d_recv,
+        a_send,
+        a_recv,
+        m_send,
+        m_recv,
+        h_send,
+        h_recv,
+        p_send,
+        p_recv,
+        w_sem,
+    ) = refs
+    n, ntp, dims, heads, attn_heads, key_heads = cfg[:6]
     me, mt = lax.axis_index("sp"), lax.axis_index("tp")
     rows, width = tokens_ref.shape
     kd = width // n
+    half = mine.shape[2]
     dcols, acols = heads * HEAD, attn_heads * HEAD
     kcols = key_heads * HEAD
 
@@ -156,44 +155,96 @@
             at = at + lax.rem(digit - o + size, size) * stride
         return at
 
-    def gather(own, buf, send, recv):
-        trees = piece_trees(dims, buf.shape[0])
+    def digit(d):
+        return lax.rem(me // dims[d][1], dims[d][0])
+
+    def gather(own, buf, send, recv, typed=False):
+        orders = piece_orders(dims, buf.shape[0])
+        lists = [arrivals(dims, order) for order in orders]
         started = []
 
-        def copy(p, node):
-            here, parent, d, step = node
+        def copy(p, parent, here, d, step):
             a, b = slot(parent), slot(here)
+            src = own[p] if a == 0 else buf.at[p, a]
+            dst = buf.at[p, b]
+            if typed and here[0] != 0:
+                size = dims[0][0]
+                if d == 0 and size > 2:
+                    kind = 0 if step > 0 else 1
+                elif d == 0:
+                    kind = digit(0)
+                else:
+                    kind = (size - 1 + here[0] - digit(0)) // size
+                src, dst = src.at[kind], dst.at[kind]
             return pltpu.make_async_remote_copy(
-                src_ref=own.at[p] if a == 0 else buf.at[p, a],
-                dst_ref=buf.at[p, b],
-                send_sem=send.at[p, b],
+                src_ref=src,
+                dst_ref=dst,
+                send_sem=send.at[p, b + (0 if step > 0 else n)],
                 recv_sem=recv.at[p, b],
-                device_id={"sp": shifted(d, step)},
+                device_id={"sp": me + step * dims[d][1] if dims[d][0] > 2 else shifted(d, 1)},
             )
 
-        def forward(p, offset):
-            for node in trees[p]:
-                if node[1] == offset:
-                    made = copy(p, node)
+        def launch(p, parent, d):
+            size, now = dims[d][0], parent[d]
+            if size == 2:
+                if now == 0:
+                    moves = [(1, None)]
+                else:
+                    moves = []
+            else:
+                at = digit(d)
+                moves = []
+                if now + 1 < size:
+                    moves.append((1, (at < size - 1) & (at >= now)))
+                if now == 0:
+                    moves.append((-1, at > 0))
+                elif now > 1:
+                    moves.append((-1, (at > 0) & (at < now)))
+            for step, when in moves:
+                here = parent[:d] + ((now + step) % size,) + parent[d + 1 :]
+                made = copy(p, parent, here, d, step)
+                if when is None:
                     made.start()
-                    started.append(made)
+                else:
+                    pl.when(when)(made.start)
+                started.append((made, when))
 
         def begin():
-            for p in range(len(trees)):
-                forward(p, (0,) * len(dims))
-
-        def arrive(index, acc):
-            for p in range(len(trees)):
-                copy(p, trees[p][index]).wait_recv()
-                forward(p, trees[p][index][0])
-            for p in range(len(trees)):
-                here = trees[p][index][0]
-                acc[p] += dot(norm3[source(here)], buf[p, slot(here)])
-
-        return begin, arrive, started
-
-    d_begin, d_arrive, d_started = gather(wd_ref, dbuf, d_send, d_recv)
-    a_begin, a_arrive, a_started = gather(wa_ref, abuf, a_send, a_recv)
+            for p, order in enumerate(orders):
+                for d in order:
+                    launch(p, (0,) * len(dims), d)
+
+        def arrive(index, use):
+            for p, order in enumerate(orders):
+                here, d = lists[p][index]
+                copy(p, here, here, d, 1).wait_recv()
+                for later in order[order.index(d) :]:
+                    launch(p, here, later)
+            if use is not None:
+                for p in range(len(orders)):
+                    here = lists[p][index][0]
+                    use[p] += dot(norm3[source(here)], buf[p, slot(here)])
+
+        def finish():
+            for made, when in started:
+                if when is None:
+                    made.wait_send()
+                else:
+                    pl.when(when)(made.wait_send)
+
+        return begin, arrive, finish
+
+    def views(weights, pieces, each):
+        if len(weights) == 1:
+            return [weights[0].at[p] for p in range(pieces)]
+        return [w.at[:, c : c + each] for w in weights for c in range(0, w.shape[1], each)]
+
+    wd_own = views(w_refs[: parts[0]], dbuf.shape[0], dbuf.shape[3])
+    wa_own = views(w_refs[parts[0] :], abuf.shape[0], abuf.shape[3])
+    m_own = [mine.at[p] for p in range(mine.shape[0])]
+    d_begin, d_arrive, d_finish = gather(wd_own, dbuf, d_send, d_recv)
+    a_begin, a_arrive, a_finish = gather(wa_own, abuf, a_send, a_recv)
+    m_begin, m_arrive, m_finish = gather(m_own, maps, m_send, m_recv, typed=True)
     d_begin()
     w_copies = [
         pltpu.make_async_copy(delta_out_hbm, wo.at[0], w_sem.at[0]),
@@ -225,10 +276,10 @@
         sums_row.append(exact_dot(decay, tri, ((1,), (1,))))
         sums_col.append(exact_dot(tri, decay, ((1,), (1,))))
         strength_col.append(exact_dot(eye, strength, ((1,), (1,))))
-    for p in range(wd_ref.shape[0]):
-        dacc[p] = dot(norm3[me], wd_ref[p])
-    for p in range(wa_ref.shape[0]):
-        aacc[p] = dot(norm3[me], wa_ref[p])
+    for p in range(dbuf.shape[0]):
+        dacc[p] = dot(norm3[me], wd_own[p][...])
+    for p in range(abuf.shape[0]):
+        aacc[p] = dot(norm3[me], wa_own[p][...])
     for index in range(n - 1):
         d_arrive(index, dacc)
     a_begin()
@@ -293,7 +344,7 @@
         for c in chains:
             mapped = dot(c["carried"], c["uw"], ((0,), (0,))) * turn
             mapped = mapped + shift_eye * jnp.exp(c["total"])
-            mine[c["r"], c["h"]] = mapped.astype(BF16)
+            mine[c["h"] // half, c["r"], c["h"] % half] = mapped.astype(BF16)
             c["read"] = dot(c["mix"], c["uw"])
         for f, b in zip(chains[::2], chains[1::2]):
             base_out[f["h"]] = f["read"][:, :HEAD] + b["read"][:, :HEAD]
@@ -311,18 +362,7 @@
             a_arrive(done, aacc)
             done += 1
 
-    m_copies = []
-    for k in range(1, n):
-        made = pltpu.make_async_remote_copy(
-            src_ref=mine.at[(me + k) // n],
-            dst_ref=maps.at[me],
-            send_sem=m_send.at[k],
-            recv_sem=m_recv.at[me],
-            device_id={"sp": lax.rem(me + k, n)},
-        )
-        made.start()
-        m_copies.append(made)
-
+    m_begin()
     while done < n - 1:
         a_arrive(done, aacc)
         done += 1
@@ -354,6 +394,7 @@
         jnp.where(ok_high, far_high, 1e30),
     ]
     share = attn_heads // key_heads
+    m_done = 0
     for h in range(attn_heads):
         at = (h // share) * HEAD
         q = prec[:, h * HEAD : (h + 1) * HEAD]
@@ -372,19 +413,22 @@
         scale = 1.0 / (total + jnp.exp(sink - top))
         res = dot(weights[0], vals[0]) + dot(weights[1], vals[1]) + dot(weights[2], vals[2])
         feats[:, dcols + h * HEAD : dcols + (h + 1) * HEAD] = (res * scale).astype(BF16)
+        while m_done < (n - 1) * (h + 1) // attn_heads:
+            m_arrive(m_done, None)
+            m_done += 1
 
     state[...] = start_ref[...]
+    while m_done < n - 1:
+        m_arrive(m_done, None)
+        m_done += 1
 
     def apply(r, s):
-        pltpu.make_async_remote_copy(
-            src_ref=mine.at[0],
-            dst_ref=maps.at[s],
-            send_sem=m_send.at[0],
-            recv_sem=m_recv.at[s],
-            device_id={"sp": lax.rem(me + 1, n)},
-        ).wait_recv()
+        at = 0
+        for size, stride in dims:
+            mine_at, there = lax.rem(me // stride, size), lax.rem(s // stride, size)
+            at = at + lax.rem(mine_at - there + size, size) * stride
         for h in range(heads):
-            m = maps[s, h]
+            m = maps[h // half, at, r, h % half]
             now = state[r, h]
             high = now.astype(BF16)
             rest = (now - high.astype(F32)).astype(BF16)
@@ -436,8 +480,11 @@
         p_copies[k - 1].wait_recv()
         total = total + partial[1, k].astype(F32)
     out_ref[...] = total.astype(BF16)
-    for made in d_started + a_started + m_copies + h_copies + p_copies:
+    for made in h_copies + p_copies:
         made.wait_send()
+    d_finish()
+    a_finish()
+    m_finish()
 
 
 def cut(weights):
@@ -473,34 +520,41 @@
     key_heads = attention_key_weight.shape[1] // HEAD
     gates = lax.dynamic_slice_in_dim(gate_weight, lax.axis_index("tp") * heads, heads, 2)
     gates = gates.reshape(gate_weight.shape[0], 4 * heads).T
-    wd = cut([delta_query_weight, delta_key_weight, delta_value_weight])
-    wa = cut([attention_query_weight, attention_key_weight, attention_value_weight])
+    wd = [delta_query_weight, delta_key_weight, delta_value_weight]
+    wa = [attention_query_weight, attention_key_weight, attention_value_weight]
+    each = key_heads * HEAD
+    if each % 128 == 0 and heads % key_heads == 0 and attn_heads % key_heads == 0:
+        pd, pa = [sum(w.shape[1] for w in some) // each for some in (wd, wa)]
+        shape_d = shape_a = (wd[0].shape[0], each)
+    else:
+        wd, wa = [cut(wd)], [cut(wa)]
+        pd, pa, shape_d, shape_a = wd[0].shape[0], wa[0].shape[0], wd[0].shape[1:], wa[0].shape[1:]
     head_ids = (lax.axis_index("tp") * attn_heads + jnp.arange(attn_heads)).astype(F32)
     slopes = jnp.exp2(-8.0 * (head_ids + 1.0) / (attn_heads * ntp))
     logits = jnp.stack([slopes, sink], axis=1)
-    cfg = (n, ntp, dims, heads, attn_heads, key_heads)
+    cfg = (n, ntp, dims, heads, attn_heads, key_heads, len(wd), len(wa))
     dcols, acols, kcols = heads * HEAD, attn_heads * HEAD, key_heads * HEAD
-    pd, pa = wd.shape[0], wa.shape[0]
+    pm = 2 if heads % 2 == 0 else 1
     vmem = pl.BlockSpec(memory_space=pltpu.VMEM)
     hbm = pl.BlockSpec(memory_space=pl.ANY)
     dma = pltpu.SemaphoreType.DMA
     return pl.pallas_call(
         functools.partial(kernel, cfg),
         out_shape=jax.ShapeDtypeStruct((rows // ntp, width), BF16),
-        in_specs=[vmem] * 10 + [hbm] * 2,
+        in_specs=[vmem] * (8 + len(wd) + len(wa)) + [hbm] * 2,
         out_specs=vmem,
         scratch_shapes=[
             pltpu.VMEM((n, rows, width // n), BF16),
-            pltpu.VMEM((pd, n) + wd.shape[1:], BF16),
-            pltpu.VMEM((pa, n) + wa.shape[1:], BF16),
-            pltpu.VMEM((pd, rows, wd.shape[2]), F32),
-            pltpu.VMEM((pa, rows, wa.shape[2]), F32),
+            pltpu.VMEM((pd, n) + shape_d, BF16),
+            pltpu.VMEM((pa, n) + shape_a, BF16),
+            pltpu.VMEM((pd, rows, shape_d[1]), F32),
+            pltpu.VMEM((pa, rows, shape_a[1]), F32),
             pltpu.VMEM((rows, 3 * dcols), BF16),
             pltpu.VMEM((8, 128), BF16),
             pltpu.VMEM((rows, 2 * kcols), BF16),
             pltpu.VMEM((2, rows, 2 * kcols), BF16),
-            pltpu.VMEM((2, heads, HEAD, 2 * HEAD), BF16),
-            pltpu.VMEM((n, heads, HEAD, 2 * HEAD), BF16),
+            pltpu.VMEM((pm, 2, heads // pm, HEAD, 2 * HEAD), BF16),
+            pltpu.VMEM((pm, n, 2, heads // pm, HEAD, 2 * HEAD), BF16),
             pltpu.VMEM((2, heads, HEAD, HEAD), F32),
             pltpu.VMEM((heads, rows, HEAD), F32),
             pltpu.VMEM((heads, rows, 2 * HEAD), BF16),
@@ -508,12 +562,12 @@
             pltpu.VMEM((2,) + delta_output_weight.shape, BF16),
             pltpu.VMEM((2, ntp, rows // ntp, width), BF16),
             pltpu.VMEM((rows, acols + 2 * kcols), BF16),
+            dma((pd, 2 * n)),
             dma((pd, n)),
-            dma((pd, n)),
+            dma((pa, 2 * n)),
             dma((pa, n)),
-            dma((pa, n)),
-            dma((n,)),
-            dma((n,)),
+            dma((pm, 2 * n)),
+            dma((pm, n)),
             dma((2,)),
             dma((2,)),
             dma((ntp,)),
@@ -532,8 +586,8 @@
         starting_state,
         delta_norm_gain.reshape(1, -1),
         logits,
-        wd,
-        wa,
+        *wd,
+        *wa,
         delta_output_weight,
         attention_output_weight,
     )

time: 189 us -> 181 us (0.958)
  the two profiles are of different devices: /device:TPU:15 before, /device:TPU:0 now
where the time goes in v2:
time: 181 us
  Pallas kernels  176 us (97%)
  local copies, waits for them, and re-layouts  4.36 us (2%)
    pallas_call x1, Pallas kernels, on_device(): pl.pallas_call(functools.partial(kernel, cfg), out_shape=jax.ShapeDtypeSt...  176 us

profile of v2, /device:TPU:0, one launch (start us, length us, event | category | flops | bytes accessed | tf_op | source)
XLA Modules:
  0.0 180.6 jit_solution(15858514869055637670)
XLA Ops:
  0.0 0.0 copy-start
  0.0 0.7 pad_maximum_fusion
  0.7 0.7 copy.20.logits_ref
  1.4 1.3 copy.19
  2.7 0.0 copy-done
  2.7 0.7 dynamic-slice_bitcast_fusion.gate_ref
  3.4 175.5 %shard_map.154 = bf16[64,2048]{1,0:T(8,128)(2,1)} custom-call(bf16[128,2048]{1,0:T(8,128)(2,1)} %tokens_ref.1, f32[1,2048]{1,0:T(1,128)} %bitcast.9, bf16[32,2048]{1,0:T(8,128)(2,1)} %dynamic-slice_bitcast_fusion.gate_ref, f32[8,2]{1,0:T(8,128)} %bitcast.8, f32[8,128]{1,0:T(8,128)} %increments_ref.1, f32[2,8,64,64]{3,2,1,0:T(8,128)} %start_ref.1, ...), custom_call_target="tpu_custom_call" | custom-call | tf_op jit(solution)/shard_map/pallas_call | solution.py:541
  178.9 1.7 copy.22
  (1 shorter events, 0.0 us)
Async XLA Ops:
  0.0 2.7 %copy-start = (bf16[2048,4,16]{0,2,1:T(8,128)(2,1)S(1)}, bf16[2048,4,16]{0,2,1:T(8,128)(2,1)}, u32[]{:S(2)}) copy-start(bf16[2048,4,16]{0,2,1:T(8,128)(2,1)} %param.21) | copy-start | bytes 786436
